TPU v7x, 256 devices: a 4x2x16 block of a 4x16x16 slice. The times are simulated.
256 devices in a mesh: grp: 2 (over y), fs: 32 (over z, core), tp: 4 (over x).
Axes of the slice: x: 4, y: 2, z: 16, core: 2. Of those that a mesh axis runs over, the one named last changes fastest.
The devices are a block of a 4x16x16 slice.
Arguments:
- tokens: bfloat16 [4096, 2048], P(('grp', 'fs')), parts along dimension 0, may hold values from -6 to 6
- routes: int32 [4096, 2], P(('grp', 'fs')), parts along dimension 0, may hold values from 0 to 3, as said below
- route_logits: float32 [4096, 2], P(('grp', 'fs')), parts along dimension 0, may hold values from -8 to 8
- gain: float32 [2048], P('fs'), may hold values from 0.1 to 1.9
- w_gate: float32 [4, 2048, 7168], P(None, 'fs', 'tp'), may hold values from -0.125 to 0.125
- w_up: float32 [4, 2048, 7168], P(None, 'fs', 'tp'), may hold values from -0.125 to 0.125
- w_down: float32 [4, 7168, 2048], P(None, 'fs', 'tp'), may hold values from -0.0625 to 0.0625
Outputs:
- gate_served: bfloat16 [8, 2048, 7168], P(('grp', 'tp'), None, 'fs'), parts along dimension 0
- up_served: bfloat16 [8, 2048, 7168], P(('grp', 'tp'), None, 'fs'), parts along dimension 0
- down_served: bfloat16 [8, 7168, 2048], P(('grp', 'tp'), 'fs'), parts along dimension 0
- mixed: bfloat16 [4096, 2048], P(('grp', 'fs'), 'tp'), parts along dimension 0
There are 2 independent parts, one for each index of `grp`. A program takes and returns all parts, laid end to end along the dimension named above; an argument that names none is the same for every part. Nothing has to cross between parts.
Inputs may be any that keep to these rules, and one draw needn't show every extreme that they name: `routes`: each row names 2 different experts; every expert is named by some row.
All inputs are finite; a program needn't handle non-finite values.
Results may differ from a plain program's by a relative error of at most 0.0085.
Values may be sent and summed in bfloat16 or wider, within the bound.
No kernel may reach another device: no remote copies, remote signals or barrier semaphores. Data moves between devices by JAX's collectives and lax.ppermute only.
A program may use at most 128 MiB of HBM per device.

v0:
```python
import jax
import jax.numpy as jnp
from jax import lax
from jax.sharding import PartitionSpec as P


def sent_together(arrays, axis, split_dim, concat_dim, along):
    ends, at = ([], 0)
    for a in arrays[:-1]:
        at += a.shape[along]
        ends.append(at)
    both = jnp.concatenate(arrays, axis=along)
    return tuple(
        jnp.split(
            lax.all_to_all(both, axis, split_axis=split_dim, concat_axis=concat_dim, tiled=True),
            ends,
            axis=along,
        )
    )


def sent_together_2(arrays, axis, dim, along):
    columns = [a.reshape(*a.shape[:along], -1) for a in arrays]
    both = jnp.concatenate(columns, axis=along)
    out, at, gathered = (lax.all_gather(both, axis, axis=dim, tiled=True), 0, [])
    for a, column in zip(arrays, columns):
        piece = out[..., at : at + column.shape[along]]
        gathered.append(piece.reshape(*piece.shape[:along], *a.shape[along:]))
        at += column.shape[along]
    return tuple(gathered)


def cut_along(array, dim, count):
    dims = array.shape
    tiles = array.reshape(*dims[:dim], count, dims[dim] // count, *dims[dim + 1 :])
    return jnp.moveaxis(tiles, dim, 0)


def sent_and_summed(array, axis, dim):
    count = lax.axis_size(axis)
    tiles = lax.all_to_all(cut_along(array, dim, count), axis, 0, 0, tiled=True)
    return jnp.sum(tiles, axis=0)


def body(tokens, routes, route_logits, gain, w_gate, w_up, w_down):
    gate_cast = (w_gate * gain[None, :, None]).astype(jnp.bfloat16)
    up_cast = (w_up * gain[None, :, None]).astype(jnp.bfloat16)
    down_cast = w_down.astype(jnp.bfloat16)
    gate_tp, up_tp, down_served = (
        lax.all_to_all(gate_cast, "tp", split_axis=0, concat_axis=2, tiled=True),
        lax.all_to_all(up_cast, "tp", split_axis=0, concat_axis=2, tiled=True),
        lax.all_to_all(down_cast, "tp", split_axis=0, concat_axis=2, tiled=True),
    )
    gate_served, up_served = sent_together((gate_tp, up_tp), "fs", 2, 1, 0)
    values = tokens.astype(jnp.float32)
    mean_square = jnp.mean(values * values, axis=-1, keepdims=True)
    normed = (values * lax.rsqrt(mean_square + 1e-06)).astype(jnp.bfloat16)
    expert_id = lax.axis_index("tp")
    first = jax.nn.sigmoid(route_logits[:, 0] - route_logits[:, 1])
    second = jax.nn.sigmoid(route_logits[:, 1] - route_logits[:, 0])
    weight_col = first * (routes[:, 0] == expert_id).astype(jnp.float32)
    weight_col = (weight_col + second * (routes[:, 1] == expert_id).astype(jnp.float32)).astype(
        jnp.bfloat16
    )
    gate_local = gate_served[0]
    up_local = up_served[0]
    piece_rows, piece_weight = sent_together_2((normed, weight_col), "fs", 0, 1)
    gate_act = jnp.dot(piece_rows, gate_local, preferred_element_type=jnp.float32)
    up_act = jnp.dot(piece_rows, up_local, preferred_element_type=jnp.float32)
    hidden_rows = jax.nn.silu(gate_act) * up_act * piece_weight[:, None].astype(jnp.float32)
    hidden = hidden_rows.astype(jnp.bfloat16)
    down_local = down_served[0]
    summed_rows = lax.psum_scatter(
        jnp.dot(hidden, down_local, preferred_element_type=jnp.float32),
        "fs",
        scatter_dimension=0,
        tiled=True,
    )
    mixed = sent_and_summed(summed_rows, "tp", 1)
    return (gate_served, up_served, down_served, mixed.astype(jnp.bfloat16))


def solution(mesh):
    return jax.shard_map(
        body,
        mesh=mesh,
        in_specs=(
            P(("grp", "fs"), None),
            P(("grp", "fs"), None),
            P(("grp", "fs"), None),
            P("fs"),
            P(None, "fs", "tp"),
            P(None, "fs", "tp"),
            P(None, "fs", "tp"),
        ),
        out_specs=(
            P(("grp", "tp"), None, "fs"),
            P(("grp", "tp"), None, "fs"),
            P(("grp", "tp"), "fs", None),
            P(("grp", "fs"), "tp"),
        ),
        check_vma=False,
    )
```

profile of v0, /device:TPU:40, one launch (start us, length us, event | category | flops | bytes accessed | tf_op | source)
XLA Modules:
  0.0 363.2 jit_solution(13875330566022918010)
XLA Ops:
  7.2 0.1 all-gather.2.cloned.1.call-start
  7.2 1.1 fusion.23
  8.4 1.1 fusion.24
  9.4 0.8 fusion.26
  10.2 0.1 copy.31
  10.3 0.7 pad_maximum_fusion.1
  11.1 0.1 all-gather.2.cloned.1.call-update
  11.1 3.3 multiply_convert_fusion.1
  14.5 18.1 %all_to_all.74 = bf16[4,64,1792]{2,1,0:T(8,128)(2,1)S(1)} all-to-all(bf16[4,64,1792]{2,1,0:T(8,128)(2,1)S(1)} %get-tuple-element.14), channel_id=1, replica_groups=mesh['grp'=2,'fs'=32,'tp'=4] {'tp'}, dimensions={0} | all-to-all | bytes 1835008 | tf_op jit(solution)/shard_map/all_to_all | solution.py:50
  32.6 3.6 all-to-all-start.1
  36.2 2.5 convert_element_type.30
  38.7 1.0 copy.40
  39.7 9.2 %all-to-all-done.1 = bf16[4,64,1792]{2,1,0:T(8,128)(2,1)S(1)} async-done(((bf16[4,64,1792]{2,1,0:T(8,128)(2,1)}), bf16[4,64,1792]{2,1,0:T(8,128)(2,1)S(1)}, u32[]{:S(2)}, u32[]{:S(2)}) %all-to-all-start.1) | async-done | bytes 917536 | tf_op jit(solution)/shard_map/all_to_all | solution.py:51
  48.9 3.6 all-to-all-start.3
  52.5 0.0 copy-start
  52.5 0.1 copy.41
  52.6 1.1 copy-done
  53.7 0.2 pad_maximum_fusion
  53.9 6.1 %copy.26 = bf16[2,64,7168]{1,0,2:T(2,128)(2,1)} copy(bf16[2,64,7168]{2,1,0:T(8,128)(2,1)S(1)} %pad_maximum_fusion) | data formatting | bytes 3670016 | tf_op jit(solution)/shard_map/concatenate | solution.py:12
  60.0 8.8 %reshape.29 = bf16[32,2,14336]{2,1,0:T(2,128)(2,1)} reshape(bf16[7168,2,64]{2,1,0:T(2,128)(2,1)} %bitcast.36) | data formatting | bytes 3670016
  68.8 0.0 all-to-all-done.3
  68.8 24.8 %all-to-all-start.2 = ((bf16[32,2,14336]{2,1,0:T(2,128)(2,1)}), bf16[32,2,14336]{2,1,0:T(2,128)(2,1)S(1)}, u32[]{:S(2)}, u32[]{:S(2)}) async-start(bf16[32,2,14336]{2,1,0:T(2,128)(2,1)} %reshape.29), calls=%async_computation.2 | async-start | bytes 3670016 | tf_op jit(solution)/shard_map/all_to_all | solution.py:15
  93.6 0.2 reduce-scatter.2.cloned.1.call-start
  93.8 0.7 copy.30
  94.6 1.1 copy.43
  95.7 83.9 %all-to-all-done.2 = bf16[32,2,14336]{2,1,0:T(2,128)(2,1)S(1)} async-done(((bf16[32,2,14336]{2,1,0:T(2,128)(2,1)}), bf16[32,2,14336]{2,1,0:T(2,128)(2,1)S(1)}, u32[]{:S(2)}, u32[]{:S(2)}) %all-to-all-start.2) | async-done | bytes 1835040 | tf_op jit(solution)/shard_map/all_to_all | solution.py:15
  179.6 3.7 %reshape.30 = bf16[7168,2,64]{2,1,0:T(2,128)(2,1)} reshape(bf16[32,2,14336]{2,1,0:T(2,128)(2,1)S(1)} %all-to-all-done.2) | data formatting | bytes 3670016
  183.4 6.3 %copy.38 = bf16[2,64,32,224]{3,2,1,0:T(8,128)(2,1)S(1)} copy(bf16[2,64,32,224]{1,0,3,2:T(2,128)(2,1)} %bitcast.37) | data formatting | bytes 3670016 | tf_op jit(solution)/shard_map/all_to_all | solution.py:15
  189.6 0.2 fusion.28
  189.8 0.6 copy.28
  190.4 0.6 copy.29
  191.0 0.0 all-gather.2.cloned.1.call-done
  191.0 1.3 convert_reduce_fusion
  192.3 7.5 %fusion.2 = f32[2048,224]{0,1:T(8,128)} fusion(bf16[2048,224]{1,0:T(8,128)(2,1)S(1)} %bitcast.43, bf16[2048,2049]{1,0:T(8,128)(2,1)} %all-gather.2.cloned.1.call-done), kind=kOutput, calls=%fused_computation.2 | convolution fusion | flops 1879048192 | bytes 11141120 | tf_op jit(solution)/shard_map/dot_general | solution.py:68
  199.7 11.4 %fusion.14 = f32[2048,2048]{1,0:T(8,128)} fusion(bf16[224,2048]{1,0:T(8,128)(2,1)} %bitcast.50, bf16[2048,224]{1,0:T(8,128)(2,1)S(1)} %bitcast.38, bf16[2048,2049]{1,0:T(8,128)(2,1)} %all-gather.2.cloned.1.call-done, f32[2048,224]{0,1:T(8,128)} %fusion.2, f32[2048]{0:T(1024)S(1)} %convert_reduce_fusion), kind=kOutput, calls=%fused_computation.7 | convolution fusion | flops 3761307648 | bytes 28844032 | tf_op jit(solution)/shard_map/dot_general | solution.py:74
  211.1 0.1 reduce-scatter.2.cloned.1.call-update
  211.2 130.5 %reduce-scatter.2.cloned.1.call-done = f32[64,2048]{1,0:T(8,128)} async-done(((f32[2048,2048]{1,0:T(8,128)}), f32[64,2048]{1,0:T(8,128)}) %reduce-scatter.2.cloned.1.call-update) | async-done | bytes 524304 | tf_op jit(solution)/shard_map/reduce_scatter | solution.py:73
  341.7 1.9 copy.45
  343.6 4.0 %all-to-all-start.4 = ((f32[4,64,512]{2,1,0:T(8,128)}), f32[4,64,512]{2,1,0:T(8,128)S(1)}, u32[]{:S(2)}, u32[]{:S(2)}) async-start(f32[4,64,512]{2,1,0:T(8,128)} %bitcast.51), calls=%async_computation.5 | async-start | bytes 1048576 | tf_op jit(solution)/shard_map/all_to_all | solution.py:41
  347.6 1.0 copy.42
  348.6 1.3 copy.36
  349.9 1.3 copy.37
  351.1 4.5 %all-to-all-done.4 = f32[4,64,512]{2,1,0:T(8,128)S(1)} async-done(((f32[4,64,512]{2,1,0:T(8,128)}), f32[4,64,512]{2,1,0:T(8,128)S(1)}, u32[]{:S(2)}, u32[]{:S(2)}) %all-to-all-start.4) | async-done | bytes 524320 | tf_op jit(solution)/shard_map/all_to_all | solution.py:41
  355.6 0.7 reduce_sum.19
  (1 shorter events, 0.0 us)
Async XLA Ops:
  7.2 183.8 %all-gather.2.cloned.1.call-start = ((), (), s32[]{:S(2)}) async-start(), calls=%async_computation.6 | async-start | bytes 9191424 | tf_op jit(solution)/shard_map/all_gather | solution.py:25
  32.6 16.3 %all-to-all-start.1 = ((bf16[4,64,1792]{2,1,0:T(8,128)(2,1)}), bf16[4,64,1792]{2,1,0:T(8,128)(2,1)S(1)}, u32[]{:S(2)}, u32[]{:S(2)}) async-start(bf16[4,64,1792]{2,1,0:T(8,128)(2,1)} %get-tuple-element.15), calls=%async_computation.1 | async-start | bytes 1835008 | tf_op jit(solution)/shard_map/all_to_all | solution.py:51
  48.9 19.9 %all-to-all-start.3 = ((bf16[4,224,512]{2,1,0:T(8,128)(2,1)}), bf16[4,224,512]{2,1,0:T(8,128)(2,1)S(1)}, u32[]{:S(2)}, u32[]{:S(2)}) async-start(bf16[4,224,512]{2,1,0:T(8,128)(2,1)} %convert_element_type.30), calls=%async_computation.3 | async-start | bytes 1835008 | tf_op jit(solution)/shard_map/all_to_all | solution.py:52
  52.5 1.2 copy-start
  68.8 110.8 %all-to-all-start.2 = ((bf16[32,2,14336]{2,1,0:T(2,128)(2,1)}), bf16[32,2,14336]{2,1,0:T(2,128)(2,1)S(1)}, u32[]{:S(2)}, u32[]{:S(2)}) async-start(bf16[32,2,14336]{2,1,0:T(2,128)(2,1)} %reshape.29), calls=%async_computation.2 | async-start | bytes 3670016 | tf_op jit(solution)/shard_map/all_to_all | solution.py:15
  93.6 248.1 %reduce-scatter.2.cloned.1.call-start = ((), (), s32[]{:S(2)}) async-start(), calls=%async_computation.7 | async-start | bytes 17301504 | tf_op jit(solution)/shard_map/reduce_scatter | solution.py:73
  343.6 12.1 %all-to-all-start.4 = ((f32[4,64,512]{2,1,0:T(8,128)}), f32[4,64,512]{2,1,0:T(8,128)S(1)}, u32[]{:S(2)}, u32[]{:S(2)}) async-start(f32[4,64,512]{2,1,0:T(8,128)} %bitcast.51), calls=%async_computation.5 | async-start | bytes 1048576 | tf_op jit(solution)/shard_map/all_to_all | solution.py:41
Sparse Core Ops, SparseCore 0:
  11.3 99.3 all-gather.1
  211.3 130.3 reduce-scatter.1
where the time goes:
time: 364 us; the launch traced here: 363 us
  waiting for transfers between devices  228 us (63%)
  starting transfers between devices  36.3 us (10%)
  local copies, waits for them, and re-layouts  35.8 us (10%)
  matrix products  18.9 us (5%)
  blocking collectives  18.1 us (5%)
  between operations  14.2 us (4%)
  other arithmetic  11.7 us (3%)
    reduce_scatter x1, waiting for transfers between devices, body(): lax.psum_scatter(jnp.dot(hidden, down_local, preferred_element_type=jnp.f...  130 us
    all_to_all x1, waiting for transfers between devices, sent_together(): lax.all_to_all(both, axis, split_axis=split_dim, concat_axis=concat_dim,...  83.9 us
    all_to_all x1, starting transfers between devices, sent_together(): lax.all_to_all(both, axis, split_axis=split_dim, concat_axis=concat_dim,...  24.8 us
    all_to_all x1, blocking collectives, body(): lax.all_to_all(gate_cast, 'tp', split_axis=0, concat_axis=2, tiled=True)  18.1 us
    unnamed x7, local copies, waits for them, and re-layouts  17.3 us
    dot_general x1, matrix products, body(): jnp.dot(hidden, down_local, preferred_element_type=jnp.float32)  11.4 us
    all_to_all x1, waiting for transfers between devices, body(): lax.all_to_all(up_cast, 'tp', split_axis=0, concat_axis=2, tiled=True)  9.15 us
    dot_general x1, matrix products, body(): jnp.dot(piece_rows, gate_local, preferred_element_type=jnp.float32)  7.47 us
  transfers between devices with their start and end apart: 6, of which 4 were waited for; matrix products, arithmetic and copies ran while one was open for 11% of the time, Pallas kernels for 0%

commit v1 on v0

v1 whole, which is shorter than its diff:
```python
import functools

import jax
import jax.numpy as jnp
from jax import lax
from jax.experimental import pallas as pl
from jax.experimental.pallas import tpu as pltpu
from jax.sharding import PartitionSpec as P

BF16, F32 = jnp.bfloat16, jnp.float32
LANES = 128
VMEM = 56 * 1024 * 1024


def params(*semantics):
    return pltpu.CompilerParams(dimension_semantics=semantics, vmem_limit_bytes=VMEM)


def pack_kernel(parts, width, scale_ref, gate_ref, up_ref, *out_refs):
    both = jnp.concatenate([gate_ref[0], up_ref[0]], axis=0)
    columns = (both.T * scale_ref[...]).astype(BF16)
    for k in range(columns.shape[0] // width):
        for out_ref, (low, size) in zip(out_refs, parts):
            at = k * width + low
            out_ref[0, k] = columns[at : at + size]


def pack(gain, w_gate, w_up, parts, width):
    experts, rows, columns = w_gate.shape
    scale = jnp.concatenate([gain, gain])[None, :]
    blocks = columns // width
    return pl.pallas_call(
        functools.partial(pack_kernel, parts, width),
        grid=(experts,),
        in_specs=[
            pl.BlockSpec((1, 2 * rows), lambda e: (0, 0)),
            pl.BlockSpec((1, rows, columns), lambda e: (e, 0, 0)),
            pl.BlockSpec((1, rows, columns), lambda e: (e, 0, 0)),
        ],
        out_specs=[
            pl.BlockSpec((1, blocks, size, 2 * rows), lambda e: (e, 0, 0, 0)) for _, size in parts
        ],
        out_shape=[
            jax.ShapeDtypeStruct((experts, blocks, size, 2 * rows), BF16) for _, size in parts
        ],
        compiler_params=params("arbitrary"),
        cost_estimate=pl.CostEstimate(
            flops=experts * rows * columns * 200, bytes_accessed=experts * rows * columns * 12, transcendentals=0
        ),
        name="pack",
    )(scale, w_gate, w_up)


def unpack_kernel(size, recv_ref, gate_ref, up_ref, both_ref):
    half = recv_ref.shape[2] // 2
    pad = both_ref.shape[0] // 2 - size
    if pad:
        zeros = jnp.zeros((pad, both_ref.shape[1]), BF16)
        both_ref[size : size + pad] = zeros
        both_ref[size + pad + size :] = zeros
    for k in range(recv_ref.shape[0] // 2):
        one, two = recv_ref[2 * k], recv_ref[2 * k + 1]
        at = slice(k * 2 * half, (k + 1) * 2 * half)
        gate = jnp.concatenate([one[:, :half], two[:, :half]], axis=1)
        up = jnp.concatenate([one[:, half:], two[:, half:]], axis=1)
        gate_ref[:, at] = gate
        up_ref[:, at] = up
        both_ref[0:size, at] = gate
        both_ref[size + pad : size + pad + size, at] = up


def unpack(recv, padded):
    count, size, lanes = recv.shape
    width = count * lanes // 2
    return pl.pallas_call(
        functools.partial(unpack_kernel, size),
        in_specs=[pl.BlockSpec(memory_space=pltpu.VMEM)],
        out_specs=[pl.BlockSpec(memory_space=pltpu.VMEM)] * 3,
        out_shape=[
            jax.ShapeDtypeStruct((size, width), BF16),
            jax.ShapeDtypeStruct((size, width), BF16),
            jax.ShapeDtypeStruct((2 * padded, width), BF16),
        ],
        compiler_params=params(),
        cost_estimate=pl.CostEstimate(flops=count * size * lanes * 40, bytes_accessed=count * size * lanes * 6, transcendentals=0),
        name="unpack",
    )(recv)


def hidden_kernel(depth, expert_ref, tokens_ref, both_ref, out_ref):
    owners, rows = tokens_ref.shape[0], tokens_ref.shape[2]
    block = tokens_ref[...].reshape(owners * rows, tokens_ref.shape[3])
    acts = lax.dot_general(
        block[:, :depth], both_ref[...], (((1,), (1,)), ((), ())), preferred_element_type=F32
    )
    shares = block[:, depth:].astype(F32)
    lane = lax.broadcasted_iota(jnp.int32, shares.shape, 1)
    share = jnp.sum(jnp.where(lane == expert_ref[0], shares, 0.0), axis=1, keepdims=True)
    half = acts.shape[1] // 2
    gate, up = acts[:, :half], acts[:, half:]
    hidden = gate / (1.0 + jnp.exp(-gate)) * up * share
    out_ref[...] = hidden.astype(BF16).reshape(1, owners, rows, half)


def hidden_of(expert, tokens, both, depth, first, count, owners):
    n_owner, _, rows, wide = tokens.shape
    half = both.shape[0] // 2
    work = count * n_owner * rows
    return pl.pallas_call(
        functools.partial(hidden_kernel, depth),
        grid=(count, n_owner // owners),
        in_specs=[
            pl.BlockSpec(memory_space=pltpu.SMEM),
            pl.BlockSpec((owners, 1, rows, wide), lambda q, i: (i, q + first, 0, 0)),
            pl.BlockSpec(both.shape, lambda q, i: (0, 0)),
        ],
        out_specs=pl.BlockSpec((1, owners, rows, half), lambda q, i: (q, i, 0, 0)),
        out_shape=jax.ShapeDtypeStruct((count, n_owner, rows, half), BF16),
        compiler_params=params("arbitrary", "arbitrary"),
        cost_estimate=pl.CostEstimate(
            flops=2 * work * depth * 2 * half, bytes_accessed=work * wide * 2 + both.size * 2, transcendentals=work * half
        ),
        name="hidden",
    )(expert, tokens, both)


def down_kernel(experts, place_ref, down_ref, *refs):
    parts, (keep_ref, send_ref) = refs[:-2], refs[-2:]
    per = len(parts) // experts
    total = None
    for shift in range(experts):
        pieces = []
        for p in range(per):
            r = parts[p * experts + shift]
            pieces.append(r[...].reshape(-1, r.shape[-1]))
        source = lax.rem(place_ref[0] + experts - shift, experts)
        left = jnp.concatenate(pieces, axis=1) if per > 1 else pieces[0]
        term = jnp.dot(left, down_ref[source], preferred_element_type=F32)
        total = term if total is None else total + term
    pairs = total.reshape(keep_ref.shape[0], 2, keep_ref.shape[1], total.shape[1])
    even, odd = pairs[:, 0], pairs[:, 1]
    mine = place_ref[1] == 0
    keep_ref[...] = jnp.where(mine, even, odd)
    send_ref[...] = jnp.where(mine, odd, even).astype(BF16)


def down_of(place, down, pieces, at, owners):
    experts, _, features = down.shape
    _, n_owner, rows, _ = pieces[0][0].shape
    flat, specs = [], []
    for p, group in enumerate(pieces):
        for piece in group:
            flat.append(piece)
            specs.append(
                pl.BlockSpec((1, owners, rows, piece.shape[3]), functools.partial(lambda q, i: (q, i, 0, 0), at[p]))
            )
    out = pl.BlockSpec((owners // 2, rows, features), lambda i: (i, 0, 0))
    return pl.pallas_call(
        functools.partial(down_kernel, experts),
        grid=(n_owner // owners,),
        in_specs=[
            pl.BlockSpec(memory_space=pltpu.SMEM),
            pl.BlockSpec(down.shape, lambda i: (0, 0, 0)),
            *specs,
        ],
        out_specs=[out, out],
        out_shape=[
            jax.ShapeDtypeStruct((n_owner // 2, rows, features), F32),
            jax.ShapeDtypeStruct((n_owner // 2, rows, features), BF16),
        ],
        compiler_params=params("arbitrary"),
        cost_estimate=pl.CostEstimate(
            flops=2 * n_owner * rows * down.size, bytes_accessed=n_owner * rows * (features * 3 + 2048), transcendentals=0
        ),
        name="down",
    )(place, down, *flat)


def around(array, axis):
    n = lax.axis_size(axis)
    got = {0: array}
    for shift in [1, n - 1, *range(2, n - 1)]:
        got[shift] = lax.ppermute(array, axis, [(i, (i + shift) % n) for i in range(n)])
    return [got[shift] for shift in range(n)]


def body(chunks, tokens, routes, route_logits, gain, w_gate, w_up, w_down):
    n_fs, n_tp = lax.axis_size("fs"), lax.axis_size("tp")
    experts, hidden_rows, features = w_down.shape
    count, depth = tokens.shape
    me = lax.axis_index("fs")
    expert = lax.axis_index("tp").astype(jnp.int32)
    parts = ((0, LANES), (LANES, hidden_rows - LANES))

    values = tokens.astype(F32)
    mean_square = jnp.mean(values * values, axis=-1, keepdims=True)
    normed = (values * lax.rsqrt(mean_square + 1e-06)).astype(BF16)
    first = jax.nn.sigmoid(route_logits[:, 0:1] - route_logits[:, 1:2])
    second = jax.nn.sigmoid(route_logits[:, 1:2] - route_logits[:, 0:1])
    names = lax.broadcasted_iota(jnp.int32, (count, LANES), 1)
    share = first * (routes[:, 0:1] == names).astype(F32)
    share = (share + second * (routes[:, 1:2] == names).astype(F32)).astype(BF16)
    rows = jnp.concatenate([normed, share], axis=1)
    gathered = lax.all_gather(rows, "fs", axis=0, tiled=True)
    gathered = gathered.reshape(n_fs, chunks, count // chunks, depth + LANES)

    packed = pack(gain, w_gate, w_up, parts, hidden_rows)
    received = []
    for piece in packed:
        e, blocks, size, lanes = piece.shape
        across = lax.all_to_all(piece.reshape(e, blocks * size, lanes), "tp", 0, 0, tiled=True)
        across = across.reshape(n_fs, size, lanes)
        received.append(lax.all_to_all(across, "fs", 0, 0, tiled=True))

    down_cast = w_down.astype(BF16)
    down_rows = lax.all_to_all(down_cast, "tp", 0, 0, tiled=True)
    down_served = jnp.swapaxes(down_rows, 0, 1).reshape(1, hidden_rows, n_tp * features)
    down_padded = jnp.pad(down_cast, ((0, 0), (0, len(parts) * LANES - hidden_rows), (0, 0)))

    place = jnp.stack([expert, (me % 2).astype(jnp.int32)])
    mine = expert[None]
    gates, ups, boths = zip(*(unpack(r, LANES) for r in received))
    early = around(hidden_of(mine, gathered, boths[0], depth, 0, chunks, 8), "tp")
    swap = [(i, i + 1 - 2 * (i % 2)) for i in range(n_fs)]
    columns = [list(range(c, n_fs, 2)) for c in range(2)]
    out = []
    for q in range(chunks):
        late = around(hidden_of(mine, gathered, boths[1], depth, q, 1, 8), "tp")
        keep, send = down_of(place, down_padded, [early, late], [q, 0], 8)
        summed = (keep + lax.ppermute(send, "fs", swap).astype(F32)).astype(BF16)
        spread = lax.all_to_all(summed, "fs", 0, 0, axis_index_groups=columns, tiled=True)
        out.append(jnp.sum(spread.astype(F32), axis=0).astype(BF16))
    mixed = jnp.concatenate(out, axis=0)
    gate_served = jnp.concatenate(gates, axis=0).T[None]
    up_served = jnp.concatenate(ups, axis=0).T[None]
    return gate_served, up_served, down_served, mixed


def solution(mesh):
    return jax.shard_map(
        functools.partial(body, 2),
        mesh=mesh,
        in_specs=(
            P(("grp", "fs"), None),
            P(("grp", "fs"), None),
            P(("grp", "fs"), None),
            P("fs"),
            P(None, "fs", "tp"),
            P(None, "fs", "tp"),
            P(None, "fs", "tp"),
        ),
        out_specs=(
            P(("grp", "tp"), None, "fs"),
            P(("grp", "tp"), None, "fs"),
            P(("grp", "tp"), "fs", None),
            P(("grp", "fs"), "tp"),
        ),
        check_vma=False,
    )
```

time: 364 us -> 357 us (0.981)
  waiting for transfers between devices: 228 us -> 132 us
  blocking collectives: 18.1 us -> 112 us
  Pallas kernels: 0 us -> 39.8 us
  local copies, waits for them, and re-layouts: 35.8 us -> 8.81 us
  matrix products: 18.9 us -> 0 us
    reduce_scatter x1 -> x0, waiting for transfers between devices: 130 us -> none  [body(): lax.psum_scatter(jnp.dot(hidden, down_local, preferred_element_type=jnp.f...]
    all_to_all x1 -> x3, blocking collectives: 18.1 us -> 112 us  [the longest x1 77.7 us: body(): received.append(lax.all_to_all(across, 'fs', 0, 0, tiled=True))]
    ppermute x0 -> x11, waiting for transfers between devices: none -> 41.6 us  [the longest x9 39.5 us: around(): lax.ppermute(array, axis, [(i, (i + shift) % n) for i in range(n)])]
    pallas_call x0 -> x8, Pallas kernels: none -> 39.8 us  [the longest x3 19.3 us: hidden_of(): pl.pallas_call(functools.partial(hidden_kernel, depth), grid=(count, n_ow...]
    dot_general x2 -> x0, matrix products: 18.9 us -> none  [the longest x1 11.4 us: body(): jnp.dot(hidden, down_local, preferred_element_type=jnp.float32)]
    unnamed x7 -> x26, local copies, waits for them, and re-layouts: 17.3 us -> 3.49 us
    all_to_all x4, starting transfers between devices: 36 us -> 24.1 us  [the longest x2 15.6 us: body(): lax.all_to_all(summed, 'fs', 0, 0, axis_index_groups=columns, tiled=True)]
    ppermute x0 -> x11, starting transfers between devices: none -> 11.1 us  [the longest x9 10.8 us: around(): lax.ppermute(array, axis, [(i, (i + shift) % n) for i in range(n)])]
  transfers between devices with their start and end apart: 6 -> 16, of which waited for: 4 -> 9; matrix products, arithmetic and copies ran while one was open for 11% -> 4% of each run, Pallas kernels for 0% -> 8%
where the time goes in v1:
time: 357 us; the launch traced here: 356 us
  waiting for transfers between devices  132 us (37%)
  blocking collectives  112 us (31%)
  Pallas kernels  39.8 us (11%)
  starting transfers between devices  35.3 us (10%)
  between operations  14.2 us (4%)
  other arithmetic  13 us (4%)
  local copies, waits for them, and re-layouts  8.81 us (2%)
    all_to_all x1, blocking collectives, body(): received.append(lax.all_to_all(across, 'fs', 0, 0, tiled=True))  77.7 us
    all_to_all x1, waiting for transfers between devices, body(): received.append(lax.all_to_all(across, 'fs', 0, 0, tiled=True))  52.9 us
    ppermute x9, waiting for transfers between devices, around(): lax.ppermute(array, axis, [(i, (i + shift) % n) for i in range(n)])  39.5 us
    all_to_all x2, blocking collectives, body(): lax.all_to_all(piece.reshape(e, blocks * size, lanes), 'tp', 0, 0, tiled=...  34.4 us
    all_to_all x2, waiting for transfers between devices, body(): lax.all_to_all(summed, 'fs', 0, 0, axis_index_groups=columns, tiled=True)  24.2 us
    pallas_call x3, Pallas kernels, hidden_of(): pl.pallas_call(functools.partial(hidden_kernel, depth), grid=(count, n_ow...  19.3 us
    all_to_all x2, starting transfers between devices, body(): lax.all_to_all(summed, 'fs', 0, 0, axis_index_groups=columns, tiled=True)  15.6 us
    all_to_all x1, waiting for transfers between devices, body(): down_rows = lax.all_to_all(down_cast, 'tp', 0, 0, tiled=True)  13.4 us
  transfers between devices with their start and end apart: 16, of which 9 were waited for; matrix products, arithmetic and copies ran while one was open for 4% of the time, Pallas kernels for 8%

profile of v1, /device:TPU:40, one launch (start us, length us, event | category | flops | bytes accessed | tf_op | source)
XLA Modules:
  0.0 355.5 jit_solution(9263752893446970804)
XLA Ops:
  7.2 0.1 all-gather.2.cloned.1.call-start
  7.2 1.1 fusion
  8.4 0.8 slice_bitcast_fusion.1
  9.1 0.8 divide_bitcast_fusion.1
  9.9 1.1 fusion.1
  11.0 0.1 add_convert_fusion.2
  11.1 0.7 pad_maximum_fusion
  11.8 0.1 all-gather.2.cloned.1.call-update
  11.9 1.3 maximum_bitcast_fusion.2.scale_ref
  13.2 4.5 %pack.1 = (bf16[4,8,128,128]{3,2,1,0:T(8,128)(2,1)}, bf16[4,8,96,128]{3,2,1,0:T(8,128)(2,1)}) custom-call(f32[1,128]{1,0:T(1,128)} %maximum_bitcast_fusion.2.scale_ref, f32[4,64,1792]{2,1,0:T(8,128)} %gate_ref.1, f32[4,64,1792]{2,1,0:T(8,128)} %up_ref.1), custom_call_target="tpu_custom_call" | custom-call | flops 91750400 | bytes 5505024 | tf_op jit(solution)/shard_map/pack/pallas_call | solution.py:32
  17.7 17.1 %all_to_all.35 = bf16[4,768,128]{2,1,0:T(8,128)(2,1)S(1)} all-to-all(bf16[4,768,128]{2,1,0:T(8,128)(2,1)} %bitcast.32), channel_id=1, replica_groups=mesh['grp'=2,'fs'=32,'tp'=4] {'tp'}, dimensions={0} | all-to-all | bytes 1572864 | tf_op jit(solution)/shard_map/all_to_all | solution.py:211
  34.8 17.4 %all_to_all.36 = bf16[4,1024,128]{2,1,0:T(8,128)(2,1)} all-to-all(bf16[4,1024,128]{2,1,0:T(8,128)(2,1)S(1)} %bitcast.31), channel_id=1, replica_groups=mesh['grp'=2,'fs'=32,'tp'=4] {'tp'}, dimensions={0} | all-to-all | bytes 2097152 | tf_op jit(solution)/shard_map/all_to_all | solution.py:211
  52.1 77.7 %all_to_all.37.recv_ref = bf16[32,96,128]{2,1,0:T(8,128)(2,1)} all-to-all(bf16[32,96,128]{2,1,0:T(8,128)(2,1)S(1)} %bitcast.30), channel_id=1, replica_groups=mesh['grp'=2,'fs'=32,'tp'=4] {'fs'}, dimensions={0} | all-to-all | bytes 1572864 | tf_op jit(solution)/shard_map/all_to_all | solution.py:213
  129.9 4.8 %all-to-all-start.1 = ((bf16[32,128,128]{2,1,0:T(8,128)(2,1)}), bf16[32,128,128]{2,1,0:T(8,128)(2,1)S(1)}, u32[]{:S(2)}, u32[]{:S(2)}) async-start(bf16[32,128,128]{2,1,0:T(8,128)(2,1)} %bitcast.2), calls=%async_computation.1 | async-start | bytes 2097152 | tf_op jit(solution)/shard_map/all_to_all | solution.py:213
  134.7 2.8 unpack.3
  137.5 52.9 %all-to-all-done.1.recv_ref = bf16[32,128,128]{2,1,0:T(8,128)(2,1)S(1)} async-done(((bf16[32,128,128]{2,1,0:T(8,128)(2,1)}), bf16[32,128,128]{2,1,0:T(8,128)(2,1)S(1)}, u32[]{:S(2)}, u32[]{:S(2)}) %all-to-all-start.1) | async-done | bytes 1048608 | tf_op jit(solution)/shard_map/all_to_all | solution.py:213
  190.4 1.0 copy-done
  191.4 3.1 unpack.2
  194.5 5.1 %hidden.5.refs_4_ = bf16[1,32,32,128]{3,2,1,0:T(8,128)(2,1)} custom-call(s32[1]{0:T(128)} %bitcast.10.expert_ref, bf16[32,2,32,2176]{3,2,1,0:T(8,128)(2,1)} %bitcast.26, bf16[256,2048]{1,0:T(8,128)(2,1)} %get-tuple-element.23.both_ref), custom_call_target="tpu_custom_call" | custom-call | flops 1073741824 | bytes 5505024 | tf_op jit(solution)/shard_map/hidden/pallas_call | solution.py:109
  199.6 1.1 collective-permute-start.9
  200.7 9.0 %hidden.3.refs_0_ = bf16[2,32,32,128]{3,2,1,0:T(8,128)(2,1)} custom-call(s32[1]{0:T(128)} %bitcast.10.expert_ref, bf16[32,2,32,2176]{3,2,1,0:T(8,128)(2,1)} %bitcast.27, bf16[256,2048]{1,0:T(8,128)(2,1)} %get-tuple-element.22.both_ref), custom_call_target="tpu_custom_call" | custom-call | flops 2147483648 | bytes 9961472 | tf_op jit(solution)/shard_map/hidden/pallas_call | solution.py:109
  209.7 0.2 collective-permute-start.2
  210.0 2.7 collective-permute-start.1
  212.7 0.0 collective-permute-start
  212.7 3.2 collective-permute-start.8
  215.9 0.9 collective-permute-start.7
  216.8 1.0 convert_element_type.32
  217.8 2.2 pad.4.down_ref
  220.1 0.6 pad_add_fusion.place_ref
  220.7 22.9 %collective-permute-done.8.refs_6_ = bf16[1,32,32,128]{3,2,1,0:T(8,128)(2,1)} collective-permute-done((bf16[1,32,32,128]{3,2,1,0:T(8,128)(2,1)}, bf16[1,32,32,128]{3,2,1,0:T(8,128)(2,1)}, u32[]{:S(2)}, u32[]{:S(2)}) %collective-permute-start.8) | collective-permute-done | bytes 262176 | tf_op jit(solution)/shard_map/ppermute | solution.py:183
  243.5 3.4 collective-permute-done.7.refs_5_
  247.0 0.0 collective-permute-done.2.refs_3_
  247.0 0.0 collective-permute-done.1.refs_2_
  247.0 0.8 copy-done.1
  247.8 0.2 copy-done.2
  248.0 0.8 copy-done.3
  248.8 5.1 %down.3 = (f32[16,32,512]{2,1,0:T(8,128)}, bf16[16,32,512]{2,1,0:T(8,128)(2,1)}) custom-call(s32[2]{0:T(128)} %pad_add_fusion.place_ref, bf16[4,256,512]{2,1,0:T(8,128)(2,1)} %pad.4.down_ref, bf16[2,32,32,128]{3,2,1,0:T(8,128)(2,1)} %hidden.3.refs_0_, bf16[2,32,32,128]{3,2,1,0:T(8,128)(2,1)} %copy-done.3, bf16[2,32,32,128]{3,2,1,0:T(8,128)(2,1)} %copy-done.2, ...), custom_call_target="tpu_custom_call" | custom-call | flops 1073741824 | bytes 3670016 | tf_op jit(solution)/shard_map/down/pallas_call | solution.py:158
  253.9 0.1 collective-permute-start.10
  254.0 3.7 %all-to-all-start.4 = ((bf16[4,224,512]{2,1,0:T(8,128)(2,1)}), bf16[4,224,512]{2,1,0:T(8,128)(2,1)S(1)}, u32[]{:S(2)}, u32[]{:S(2)}) async-start(bf16[4,224,512]{2,1,0:T(8,128)(2,1)} %convert_element_type.32), calls=%async_computation.4 | async-start | bytes 1835008 | tf_op jit(solution)/shard_map/all_to_all | solution.py:216
  257.8 1.0 add_convert_fusion
  258.7 13.4 %all-to-all-done.4 = bf16[4,224,512]{2,1,0:T(8,128)(2,1)S(1)} async-done(((bf16[4,224,512]{2,1,0:T(8,128)(2,1)}), bf16[4,224,512]{2,1,0:T(8,128)(2,1)S(1)}, u32[]{:S(2)}, u32[]{:S(2)}) %all-to-all-start.4) | async-done | bytes 917536 | tf_op jit(solution)/shard_map/all_to_all | solution.py:216
  272.1 4.0 %all-to-all-start.6 = ((bf16[16,32,512]{2,1,0:T(8,128)(2,1)}), bf16[16,32,512]{2,1,0:T(8,128)(2,1)S(1)}, u32[]{:S(2)}, u32[]{:S(2)}) async-start(bf16[16,32,512]{2,1,0:T(8,128)(2,1)} %add_convert_fusion), calls=%async_computation.6 | async-start | bytes 1048576 | tf_op jit(solution)/shard_map/all_to_all | solution.py:231
  276.1 5.2 %hidden.4.refs_4_ = bf16[1,32,32,128]{3,2,1,0:T(8,128)(2,1)} custom-call(s32[1]{0:T(128)} %bitcast.10.expert_ref, bf16[32,2,32,2176]{3,2,1,0:T(8,128)(2,1)} %bitcast.28, bf16[256,2048]{1,0:T(8,128)(2,1)} %get-tuple-element.23.both_ref), custom_call_target="tpu_custom_call" | custom-call | flops 1073741824 | bytes 5505024 | tf_op jit(solution)/shard_map/hidden/pallas_call | solution.py:109
  281.3 1.2 collective-permute-start.5
  282.5 1.5 collective-permute-start.4
  284.0 0.0 collective-permute-start.3
  284.0 6.7 %collective-permute-done.5.refs_7_ = bf16[1,32,32,128]{3,2,1,0:T(8,128)(2,1)S(1)} collective-permute-done((bf16[1,32,32,128]{3,2,1,0:T(8,128)(2,1)}, bf16[1,32,32,128]{3,2,1,0:T(8,128)(2,1)S(1)}, u32[]{:S(2)}, u32[]{:S(2)}) %collective-permute-start.5) | collective-permute-done | bytes 262176 | tf_op jit(solution)/shard_map/ppermute | solution.py:183
  290.7 2.7 collective-permute-done.4.refs_6_
  293.4 3.8 %collective-permute-done.3.refs_5_ = bf16[1,32,32,128]{3,2,1,0:T(8,128)(2,1)S(1)} collective-permute-done((bf16[1,32,32,128]{3,2,1,0:T(8,128)(2,1)}, bf16[1,32,32,128]{3,2,1,0:T(8,128)(2,1)S(1)}, u32[]{:S(2)}, u32[]{:S(2)}) %collective-permute-start.3) | collective-permute-done | bytes 262176 | tf_op jit(solution)/shard_map/ppermute | solution.py:183
  297.2 0.7 copy-done.12
  297.9 5.0 %down.2 = (f32[16,32,512]{2,1,0:T(8,128)}, bf16[16,32,512]{2,1,0:T(8,128)(2,1)}) custom-call(s32[2]{0:T(128)} %pad_add_fusion.place_ref, bf16[4,256,512]{2,1,0:T(8,128)(2,1)} %pad.4.down_ref, bf16[2,32,32,128]{3,2,1,0:T(8,128)(2,1)} %hidden.3.refs_0_, bf16[2,32,32,128]{3,2,1,0:T(8,128)(2,1)} %copy-done.3, bf16[2,32,32,128]{3,2,1,0:T(8,128)(2,1)} %copy-done.2, ...), custom_call_target="tpu_custom_call" | custom-call | flops 1073741824 | bytes 3670016 | tf_op jit(solution)/shard_map/down/pallas_call | solution.py:158
  302.9 0.1 collective-permute-start.6
  303.1 2.1 collective-permute-done.6
  305.2 2.2 add_convert_fusion.1
  307.4 11.5 %all-to-all-start.5 = ((bf16[16,32,512]{2,1,0:T(8,128)(2,1)}), bf16[16,32,512]{2,1,0:T(8,128)(2,1)S(1)}, u32[]{:S(2)}, u32[]{:S(2)}) async-start(bf16[16,32,512]{2,1,0:T(8,128)(2,1)} %add_convert_fusion.1), calls=%async_computation.5 | async-start | bytes 1048576 | tf_op jit(solution)/shard_map/all_to_all | solution.py:231
  318.9 0.0 copy-start.7
  318.9 0.7 copy.11
  319.7 0.0 copy-start.8
  319.7 1.6 reshape.38
  321.3 2.4 maximum_bitcast_fusion
  323.6 0.1 reduce_sum.35
  323.7 24.2 %all-to-all-done.5 = bf16[16,32,512]{2,1,0:T(8,128)(2,1)S(1)} async-done(((bf16[16,32,512]{2,1,0:T(8,128)(2,1)}), bf16[16,32,512]{2,1,0:T(8,128)(2,1)S(1)}, u32[]{:S(2)}, u32[]{:S(2)}) %all-to-all-start.5) | async-done | bytes 524320 | tf_op jit(solution)/shard_map/all_to_all | solution.py:231
  347.9 0.1 reduce_sum.34
  348.0 0.6 pad_maximum_fusion.1
  (25 shorter events, 0.1 us)
Async XLA Ops:
  7.2 187.3 %all-gather.2.cloned.1.call-start = ((), (), s32[]{:S(2)}) async-start(), calls=%async_computation.7 | async-start | bytes 9191424 | tf_op jit(solution)/shard_map/all_gather | solution.py:204
  17.7 17.1 %copy-start.6 = (bf16[4,8,128,128]{3,2,1,0:T(8,128)(2,1)S(1)}, bf16[4,8,128,128]{3,2,1,0:T(8,128)(2,1)}, u32[]{:S(2)}) copy-start(bf16[4,8,128,128]{3,2,1,0:T(8,128)(2,1)} %get-tuple-element.16) | copy-start | bytes 3145732
  129.9 60.6 %all-to-all-start.1 = ((bf16[32,128,128]{2,1,0:T(8,128)(2,1)}), bf16[32,128,128]{2,1,0:T(8,128)(2,1)S(1)}, u32[]{:S(2)}, u32[]{:S(2)}) async-start(bf16[32,128,128]{2,1,0:T(8,128)(2,1)} %bitcast.2), calls=%async_computation.1 | async-start | bytes 2097152 | tf_op jit(solution)/shard_map/all_to_all | solution.py:213
  190.4 1.0 copy-start
  199.6 16.3 %collective-permute-start.9 = (bf16[1,32,32,128]{3,2,1,0:T(8,128)(2,1)}, bf16[1,32,32,128]{3,2,1,0:T(8,128)(2,1)}, u32[]{:S(2)}, u32[]{:S(2)}) collective-permute-start(bf16[1,32,32,128]{3,2,1,0:T(8,128)(2,1)} %hidden.5.refs_4_), channel_id=1, source_target_pairs={{0,3},{1,0},{2,1},{3,2},{4,7},{5,4},{6,5},{7,6},{8,11},{9,8},{10,9... | collective-permute-start | bytes 786440 | tf_op jit(solution)/shard_map/ppermute | solution.py:183
  200.7 16.1 %copy-start.4 = (f32[4,224,512]{2,1,0:T(8,128)S(1)}, f32[4,224,512]{2,1,0:T(8,128)}, u32[]{:S(2)}) copy-start(f32[4,224,512]{2,1,0:T(8,128)} %param.13) | copy-start | bytes 5505028
  209.7 37.2 %collective-permute-start.2 = (bf16[2,32,32,128]{3,2,1,0:T(8,128)(2,1)}, bf16[2,32,32,128]{3,2,1,0:T(8,128)(2,1)S(1)}, u32[]{:S(2)}, u32[]{:S(2)}) collective-permute-start(bf16[2,32,32,128]{3,2,1,0:T(8,128)(2,1)} %hidden.3.refs_0_), channel_id=1, source_target_pairs={{0,3},{1,0},{2,1},{3,2},{4,7},{5,4},{6,5},{7,6},{8,11},{9,8},{10,9... | collective-permute-start | bytes 1572872 | tf_op jit(solution)/shard_map/ppermute | solution.py:183
  210.0 37.0 %collective-permute-start.1 = (bf16[2,32,32,128]{3,2,1,0:T(8,128)(2,1)}, bf16[2,32,32,128]{3,2,1,0:T(8,128)(2,1)S(1)}, u32[]{:S(2)}, u32[]{:S(2)}) collective-permute-start(bf16[2,32,32,128]{3,2,1,0:T(8,128)(2,1)} %hidden.3.refs_0_), channel_id=1, source_target_pairs={{0,2},{1,3},{2,0},{3,1},{4,6},{5,7},{6,4},{7,5},{8,10},{9,11},{10,... | collective-permute-start | bytes 1572872 | tf_op jit(solution)/shard_map/ppermute | solution.py:183
  212.7 34.3 %collective-permute-start = (bf16[2,32,32,128]{3,2,1,0:T(8,128)(2,1)}, bf16[2,32,32,128]{3,2,1,0:T(8,128)(2,1)S(1)}, u32[]{:S(2)}, u32[]{:S(2)}) collective-permute-start(bf16[2,32,32,128]{3,2,1,0:T(8,128)(2,1)} %hidden.3.refs_0_), channel_id=1, source_target_pairs={{0,1},{1,2},{2,3},{3,0},{4,5},{5,6},{6,7},{7,4},{8,9},{9,10},{10,1... | collective-permute-start | bytes 1572872 | tf_op jit(solution)/shard_map/ppermute | solution.py:183
  212.7 30.8 %collective-permute-start.8 = (bf16[1,32,32,128]{3,2,1,0:T(8,128)(2,1)}, bf16[1,32,32,128]{3,2,1,0:T(8,128)(2,1)}, u32[]{:S(2)}, u32[]{:S(2)}) collective-permute-start(bf16[1,32,32,128]{3,2,1,0:T(8,128)(2,1)} %hidden.5.refs_4_), channel_id=1, source_target_pairs={{0,2},{1,3},{2,0},{3,1},{4,6},{5,7},{6,4},{7,5},{8,10},{9,11},{10,... | collective-permute-start | bytes 786440 | tf_op jit(solution)/shard_map/ppermute | solution.py:183
  215.9 31.1 %collective-permute-start.7 = (bf16[1,32,32,128]{3,2,1,0:T(8,128)(2,1)}, bf16[1,32,32,128]{3,2,1,0:T(8,128)(2,1)}, u32[]{:S(2)}, u32[]{:S(2)}) collective-permute-start(bf16[1,32,32,128]{3,2,1,0:T(8,128)(2,1)} %hidden.5.refs_4_), channel_id=1, source_target_pairs={{0,1},{1,2},{2,3},{3,0},{4,5},{5,6},{6,7},{7,4},{8,9},{9,10},{10,1... | collective-permute-start | bytes 786440 | tf_op jit(solution)/shard_map/ppermute | solution.py:183
  247.0 0.8 copy-start.1
  247.0 1.0 copy-start.2
  248.0 0.8 copy-start.3
  253.8 3.9 %copy-start.5 = (f32[16,32,512]{2,1,0:T(8,128)S(1)}, f32[16,32,512]{2,1,0:T(8,128)}, u32[]{:S(2)}) copy-start(f32[16,32,512]{2,1,0:T(8,128)} %get-tuple-element.26) | copy-start | bytes 3145732
  253.9 3.9 %collective-permute-start.10 = (bf16[16,32,512]{2,1,0:T(8,128)(2,1)}, bf16[16,32,512]{2,1,0:T(8,128)(2,1)S(1)}, u32[]{:S(2)}, u32[]{:S(2)}) collective-permute-start(bf16[16,32,512]{2,1,0:T(8,128)(2,1)} %get-tuple-element.27), channel_id=1, source_target_pairs={{0,4},{4,0},{8,12},{12,8},{16,20},{20,16},{24,28},{28,24},{32,36},... | collective-permute-start | bytes 1572872 | tf_op jit(solution)/shard_map/ppermute | solution.py:230
  254.0 18.1 %all-to-all-start.4 = ((bf16[4,224,512]{2,1,0:T(8,128)(2,1)}), bf16[4,224,512]{2,1,0:T(8,128)(2,1)S(1)}, u32[]{:S(2)}, u32[]{:S(2)}) async-start(bf16[4,224,512]{2,1,0:T(8,128)(2,1)} %convert_element_type.32), calls=%async_computation.4 | async-start | bytes 1835008 | tf_op jit(solution)/shard_map/all_to_all | solution.py:216
  272.1 35.2 %all-to-all-start.6 = ((bf16[16,32,512]{2,1,0:T(8,128)(2,1)}), bf16[16,32,512]{2,1,0:T(8,128)(2,1)S(1)}, u32[]{:S(2)}, u32[]{:S(2)}) async-start(bf16[16,32,512]{2,1,0:T(8,128)(2,1)} %add_convert_fusion), calls=%async_computation.6 | async-start | bytes 1048576 | tf_op jit(solution)/shard_map/all_to_all | solution.py:231
  281.3 9.4 %collective-permute-start.5 = (bf16[1,32,32,128]{3,2,1,0:T(8,128)(2,1)}, bf16[1,32,32,128]{3,2,1,0:T(8,128)(2,1)S(1)}, u32[]{:S(2)}, u32[]{:S(2)}) collective-permute-start(bf16[1,32,32,128]{3,2,1,0:T(8,128)(2,1)} %hidden.4.refs_4_), channel_id=1, source_target_pairs={{0,3},{1,0},{2,1},{3,2},{4,7},{5,4},{6,5},{7,6},{8,11},{9,8},{10,9... | collective-permute-start | bytes 786440 | tf_op jit(solution)/shard_map/ppermute | solution.py:183
  282.5 10.9 %collective-permute-start.4 = (bf16[1,32,32,128]{3,2,1,0:T(8,128)(2,1)}, bf16[1,32,32,128]{3,2,1,0:T(8,128)(2,1)S(1)}, u32[]{:S(2)}, u32[]{:S(2)}) collective-permute-start(bf16[1,32,32,128]{3,2,1,0:T(8,128)(2,1)} %hidden.4.refs_4_), channel_id=1, source_target_pairs={{0,2},{1,3},{2,0},{3,1},{4,6},{5,7},{6,4},{7,5},{8,10},{9,11},{10,... | collective-permute-start | bytes 786440 | tf_op jit(solution)/shard_map/ppermute | solution.py:183
  284.0 13.2 %collective-permute-start.3 = (bf16[1,32,32,128]{3,2,1,0:T(8,128)(2,1)}, bf16[1,32,32,128]{3,2,1,0:T(8,128)(2,1)S(1)}, u32[]{:S(2)}, u32[]{:S(2)}) collective-permute-start(bf16[1,32,32,128]{3,2,1,0:T(8,128)(2,1)} %hidden.4.refs_4_), channel_id=1, source_target_pairs={{0,1},{1,2},{2,3},{3,0},{4,5},{5,6},{6,7},{7,4},{8,9},{9,10},{10,1... | collective-permute-start | bytes 786440 | tf_op jit(solution)/shard_map/ppermute | solution.py:183
  290.7 6.5 %copy-start.10 = (bf16[1,32,32,128]{3,2,1,0:T(8,128)(2,1)}, bf16[1,32,32,128]{3,2,1,0:T(8,128)(2,1)S(1)}, u32[]{:S(2)}) copy-start(bf16[1,32,32,128]{3,2,1,0:T(8,128)(2,1)S(1)} %collective-permute-done.5.refs_7_) | copy-start | bytes 786436
  293.4 3.8 %copy-start.11 = (bf16[1,32,32,128]{3,2,1,0:T(8,128)(2,1)}, bf16[1,32,32,128]{3,2,1,0:T(8,128)(2,1)S(1)}, u32[]{:S(2)}) copy-start(bf16[1,32,32,128]{3,2,1,0:T(8,128)(2,1)S(1)} %collective-permute-done.4.refs_6_) | copy-start | bytes 786436
  297.2 0.7 copy-start.12
  302.9 2.2 collective-permute-start.6
  307.4 40.6 %all-to-all-start.5 = ((bf16[16,32,512]{2,1,0:T(8,128)(2,1)}), bf16[16,32,512]{2,1,0:T(8,128)(2,1)S(1)}, u32[]{:S(2)}, u32[]{:S(2)}) async-start(bf16[16,32,512]{2,1,0:T(8,128)(2,1)} %add_convert_fusion.1), calls=%async_computation.5 | async-start | bytes 1048576 | tf_op jit(solution)/shard_map/all_to_all | solution.py:231
  318.9 2.4 copy-start.7
  319.7 1.6 copy-start.8
  319.7 1.6 copy-start.9
Sparse Core Ops, SparseCore 0:
  12.0 121.2 all-gather.1
